TPU v7x, 256 devices: a 8x8x2 block of a 8x8x16 slice. The times are simulated.
256 devices in a mesh: grp: 2 (over z), ep: 64 (over y, x), tp: 2 (over core).
Axes of the slice: x: 8, y: 8, z: 2, core: 2. Of those that a mesh axis runs over, the one named last changes fastest.
The devices are a block of a 8x8x16 slice.
Arguments:
- tokens_in: bfloat16 [8192, 2048], P(('grp', 'ep')), parts along dimension 0, may hold values from -6 to 6
- norm_gain: float32 [2048], replicated, may hold values from 0.1 to 1.9
- gate_proj: bfloat16 [64, 2048, 1024], P('ep', None, 'tp'), may hold values from -0.125 to 0.125
- up_proj: bfloat16 [64, 2048, 1024], P('ep', None, 'tp'), may hold values from -0.125 to 0.125
- down_proj: bfloat16 [64, 1024, 2048], P('ep', 'tp'), may hold values from -0.1875 to 0.1875
- route_ids: int32 [8192, 8], P(('grp', 'ep')), parts along dimension 0, may hold values from 0 to 63, all different within a row; in each aligned block of 64 rows (0 to 63, 64 to 127, ...) at most 16 rows name the same one
- group_weight: float32 [8192, 8], P(('grp', 'ep')), parts along dimension 0, may hold values from 0.05 to 1
- expert_weight: float32 [8192, 8], P(('grp', 'ep')), parts along dimension 0, may hold values from 0.05 to 1
Outputs:
- expert_mix: bfloat16 [8192, 2048], P(('grp', 'ep'), 'tp'), parts along dimension 0
There are 2 independent parts, one for each index of `grp`. A program takes and returns all parts, laid end to end along the dimension named above; an argument that names none is the same for every part. Nothing has to cross between parts.
Inputs may be any that keep to these rules, and one draw needn't show every extreme that they name: `route_ids`: each row names 8 different experts; within the rows of one index of ep no expert is named by more than 16 rows, a bound that some of them reach.
All inputs are finite; a program needn't handle non-finite values.
Results may differ from a plain program's by a relative error of at most 0.0077.
Values may be sent and summed in bfloat16 or wider, within the bound.
A program may use at most 64 MiB of HBM per device.

v0:
```python
import jax
import jax.numpy as jnp
from jax import lax
from jax.sharding import PartitionSpec as P

TOP = 8
EXP_GRP = 8
EPSILON = 1e-06


def cut_along(array, dim, size):
    lengths = array.shape
    blocks = array.reshape(*lengths[:dim], size, lengths[dim] // size, *lengths[dim + 1 :])
    return jnp.moveaxis(blocks, dim, 0)


def sum_at_owner(array, axis, dim):
    size = lax.axis_size(axis)
    blocks = lax.all_to_all(cut_along(array, dim, size), axis, 0, 0, tiled=True)
    return jnp.sum(blocks.astype(jnp.float32), axis=0)


def on_device(
    tokens_in, norm_gain, gate_proj, up_proj, down_proj, route_ids, group_weight, expert_weight
):
    token_count, model_width = tokens_in.shape
    expert_count = gate_proj.shape[0] * lax.axis_size("ep")
    lane_count = lax.axis_size("tp")
    part_width = model_width // lane_count
    capacity = min(token_count, max(2, 2 * token_count * TOP // expert_count))
    slot_total = expert_count * capacity
    row_values = tokens_in.astype(jnp.float32)
    inv_scale = lax.rsqrt(jnp.mean(row_values * row_values, axis=-1, keepdims=True) + EPSILON)
    normed = (row_values * inv_scale * norm_gain).astype(jnp.bfloat16)
    route_count = token_count * TOP
    flat_ids = route_ids.reshape(route_count)
    positions = jnp.arange(route_count, dtype=jnp.int32)
    same_expert = (flat_ids[:, None] == flat_ids[None, :]) & (
        positions[None, :] < positions[:, None]
    )
    slot_rank = jnp.sum(same_expert.astype(jnp.int32), axis=1)
    slot_index = flat_ids * capacity + slot_rank
    slot_match = jnp.arange(slot_total, dtype=jnp.int32)[:, None] == slot_index[None, :]
    selector = jnp.sum(
        slot_match.reshape(slot_total, token_count, TOP).astype(jnp.int32), axis=2
    ).astype(jnp.bfloat16)
    gate_local = gate_proj[0]
    up_local = up_proj[0]
    lane_index = lax.axis_index("tp")
    own_half = lax.dynamic_slice_in_dim(normed, lane_index * part_width, part_width, 1)
    outgoing = jnp.dot(selector, own_half, preferred_element_type=jnp.float32).astype(jnp.bfloat16)
    arrived = lax.all_to_all(
        outgoing.reshape(expert_count, capacity, part_width),
        "ep",
        split_axis=0,
        concat_axis=0,
        tiled=True,
    )
    arrived = arrived.reshape(slot_total, part_width)
    column_piece = lax.all_gather(arrived, "tp", axis=1, tiled=True)
    gate_acts = jnp.dot(column_piece, gate_local, preferred_element_type=jnp.float32)
    up_acts = jnp.dot(column_piece, up_local, preferred_element_type=jnp.float32)
    hidden = (jax.nn.silu(gate_acts) * up_acts).astype(jnp.bfloat16)
    partial_rows = jnp.dot(hidden, down_proj[0], preferred_element_type=jnp.float32)
    summed = sum_at_owner(
        partial_rows.reshape(expert_count, capacity, model_width).astype(jnp.bfloat16), "tp", 2
    )
    results = summed.astype(jnp.bfloat16)
    returned = lax.all_to_all(results, "ep", split_axis=0, concat_axis=0, tiled=True).reshape(
        slot_total, part_width
    )
    picked = returned[slot_index].astype(jnp.float32).reshape(token_count, TOP, part_width)
    group_ids = route_ids // EXP_GRP
    group_count = group_weight.shape[1]
    group_match = (
        group_ids[:, :, None] == jnp.arange(group_count, dtype=jnp.int32)[None, None, :]
    ).astype(jnp.float32)
    group_part = jnp.sum(group_weight[:, None, :] * group_match, axis=2)
    gate_values = group_part * expert_weight / jnp.sum(expert_weight, axis=1, keepdims=True)
    return jnp.sum(picked * gate_values[:, :, None], axis=1).astype(jnp.bfloat16)


def solution(mesh):
    in_specs = (
        P(("grp", "ep"), None),
        P(),
        P("ep", None, "tp"),
        P("ep", None, "tp"),
        P("ep", "tp", None),
        P(("grp", "ep"), None),
        P(("grp", "ep"), None),
        P(("grp", "ep"), None),
    )
    out_specs = P(("grp", "ep"), "tp")
    return jax.shard_map(
        on_device, mesh=mesh, in_specs=in_specs, out_specs=out_specs, check_vma=False
    )
```

profile of v0, /device:TPU:514, one launch (start us, length us, event | category | flops | bytes accessed | tf_op | source)
XLA Modules:
  0.0 216.0 jit_solution(7506265072580166607)
XLA Ops:
  6.5 0.0 copy-start
  6.6 0.0 all-gather.2.cloned.1.call-start
  6.6 1.1 convert_element_type.40
  7.7 1.1 multiply_reduce_fusion
  8.8 0.8 copy.24
  9.6 0.1 eq.43
  9.7 0.3 convert_reduce_fusion.1
  9.9 0.1 reduce_sum.71
  10.0 0.7 convert_reduce_fusion
  10.7 0.7 dynamic-slice
  11.4 0.8 convolution_convert_fusion.1
  12.2 72.0 %all_to_all.15 = bf16[64,16,1024]{2,1,0:T(8,128)(2,1)} all-to-all(bf16[64,16,1024]{2,1,0:T(8,128)(2,1)S(1)} %bitcast.33), channel_id=1, replica_groups=mesh['grp'=2,'ep'=64,'tp'=2] {'ep'}, dimensions={0} | all-to-all | bytes 4194304 | tf_op jit(solution)/shard_map/all_to_all | solution.py:52
  84.2 0.1 all-gather.2.cloned.1.call-update
  84.2 28.4 %all-gather.2.cloned.1.call-done = bf16[1024,2048]{1,0:T(8,128)(2,1)} async-done(((bf16[1024,1024]{1,0:T(8,128)(2,1)}), bf16[1024,2048]{1,0:T(8,128)(2,1)}) %all-gather.2.cloned.1.call-update) | async-done | bytes 4194320 | tf_op jit(solution)/shard_map/all_gather | solution.py:60
  112.7 5.3 %fusion.2 = f32[1024,512]{1,0:T(8,128)S(1)} fusion(bf16[1024,2048]{1,0:T(8,128)(2,1)} %all-gather.2.cloned.1.call-done, bf16[1,2048,512]{2,1,0:T(8,128)(2,1)} %param.11), kind=kOutput, calls=%fused_computation.6 | convolution fusion | flops 2147483648 | bytes 8388608 | tf_op jit(solution)/shard_map/dot_general | solution.py:62
  118.0 0.0 copy-done.4
  118.0 0.0 copy-done.5
  118.0 2.6 %multiply_convert_fusion = bf16[1024,512]{1,0:T(8,128)(2,1)S(1)} fusion(f32[1024,512]{1,0:T(8,128)S(1)} %fusion.2, bf16[1024,2048]{1,0:T(8,128)(2,1)S(1)} %copy-done.4, bf16[1,2048,512]{2,1,0:T(8,128)(2,1)S(1)} %copy-done.5), kind=kOutput, calls=%fused_computation.10 | convolution fusion | flops 2150629376 | bytes 9437184 | tf_op jit(solution)/shard_map/dot_general | solution.py:61
  120.6 0.0 copy-done
  120.7 2.3 %convolution_convert_fusion = bf16[64,16,2048]{2,1,0:T(8,128)(2,1)S(1)} fusion(bf16[64,16,512]{2,1,0:T(8,128)(2,1)S(1)} %bitcast.37, bf16[1,512,2048]{2,1,0:T(8,128)(2,1)S(1)} %copy-done), kind=kOutput, calls=%fused_computation.2 | convolution fusion | flops 2149580800 | bytes 7340032 | tf_op jit(solution)/shard_map/dot_general | solution.py:64
  123.0 0.6 copy.30
  123.7 8.2 %all_to_all.16 = bf16[2,64,16,1024]{3,2,1,0:T(8,128)(2,1)} all-to-all(bf16[2,64,16,1024]{3,2,1,0:T(8,128)(2,1)S(1)} %bitcast.31), channel_id=1, replica_groups=mesh['grp'=2,'ep'=64,'tp'=2] {'tp'}, dimensions={0} | all-to-all | bytes 8388608 | tf_op jit(solution)/shard_map/all_to_all | solution.py:19
  131.8 5.2 %reduce_sum.74 = bf16[64,16,1024]{2,1,0:T(8,128)(2,1)} reduce(bf16[2,64,16,1024]{3,2,1,0:T(8,128)(2,1)} %all_to_all.16, bf16[]{:T(256)} %constant.37.clone.1), dimensions={0}, to_apply=%region_3.4 | reduce | flops 1048576 | bytes 6291458 | tf_op jit(solution)/shard_map/reduce_sum | solution.py:20
  137.1 13.9 %all-to-all-start.2 = ((bf16[64,16,1024]{2,1,0:T(8,128)(2,1)}), bf16[64,16,1024]{2,1,0:T(8,128)(2,1)}, u32[]{:S(2)}, u32[]{:S(2)}) async-start(bf16[64,16,1024]{2,1,0:T(8,128)(2,1)} %reduce_sum.74), calls=%async_computation.2 | async-start | bytes 4194304 | tf_op jit(solution)/shard_map/all_to_all | solution.py:69
  150.9 0.1 mul.78
  151.0 0.0 copy-done.1
  151.1 0.0 copy-done.2
  151.1 0.0 copy-done.3
  151.1 0.1 copy.27
  151.2 51.9 %all-to-all-done.2 = bf16[64,16,1024]{2,1,0:T(8,128)(2,1)} async-done(((bf16[64,16,1024]{2,1,0:T(8,128)(2,1)}), bf16[64,16,1024]{2,1,0:T(8,128)(2,1)}, u32[]{:S(2)}, u32[]{:S(2)}) %all-to-all-start.2) | async-done | bytes 2097184 | tf_op jit(solution)/shard_map/all_to_all | solution.py:69
  203.2 4.6 %gather_fusion = bf16[512,1024]{1,0:T(8,128)(2,1)S(1)} fusion(bf16[1024,1024]{1,0:T(8,128)(2,1)} %bitcast.8, s32[1024]{0:T(1024)S(1)} %pad_clamp_fusion), kind=kCustom, calls=%fused_computation | custom fusion | bytes 2099200 | tf_op jit(solution)/shard_map/gather | solution.py:72
  207.8 1.4 fusion
  (13 shorter events, 0.1 us)
Async XLA Ops:
  6.5 114.1 %copy-start = (bf16[1,512,2048]{2,1,0:T(8,128)(2,1)S(1)}, bf16[1,512,2048]{2,1,0:T(8,128)(2,1)}, u32[]{:S(2)}) copy-start(bf16[1,512,2048]{2,1,0:T(8,128)(2,1)} %param.12) | copy-start | bytes 6291460
  6.6 106.1 %all-gather.2.cloned.1.call-start = ((), (), s32[]{:S(2)}) async-start(), calls=%async_computation.3 | async-start | bytes 6291456 | tf_op jit(solution)/shard_map/all_gather | solution.py:60
  112.6 5.3 %copy-start.4 = (bf16[1024,2048]{1,0:T(8,128)(2,1)S(1)}, bf16[1024,2048]{1,0:T(8,128)(2,1)}, u32[]{:S(2)}) copy-start(bf16[1024,2048]{1,0:T(8,128)(2,1)} %all-gather.2.cloned.1.call-done) | copy-start | bytes 12582916
  112.6 5.3 %copy-start.5 = (bf16[1,2048,512]{2,1,0:T(8,128)(2,1)S(1)}, bf16[1,2048,512]{2,1,0:T(8,128)(2,1)}, u32[]{:S(2)}) copy-start(bf16[1,2048,512]{2,1,0:T(8,128)(2,1)} %param.10) | copy-start | bytes 6291460
  137.1 14.0 %copy-start.1 = (f32[64,8]{0,1:T(8,128)S(1)}, f32[64,8]{0,1:T(8,128)}, u32[]{:S(2)}) copy-start(f32[64,8]{0,1:T(8,128)} %param.15) | copy-start | bytes 6148
  137.1 14.0 %copy-start.2 = (s32[64,8]{0,1:T(8,128)S(1)}, s32[64,8]{0,1:T(8,128)}, u32[]{:S(2)}) copy-start(s32[64,8]{0,1:T(8,128)} %param.13) | copy-start | bytes 6148
  137.1 14.0 %copy-start.3 = (f32[64,8]{0,1:T(8,128)S(1)}, f32[64,8]{0,1:T(8,128)}, u32[]{:S(2)}) copy-start(f32[64,8]{0,1:T(8,128)} %param.14) | copy-start | bytes 6148
  137.1 66.1 %all-to-all-start.2 = ((bf16[64,16,1024]{2,1,0:T(8,128)(2,1)}), bf16[64,16,1024]{2,1,0:T(8,128)(2,1)}, u32[]{:S(2)}, u32[]{:S(2)}) async-start(bf16[64,16,1024]{2,1,0:T(8,128)(2,1)} %reduce_sum.74), calls=%async_computation.2 | async-start | bytes 4194304 | tf_op jit(solution)/shard_map/all_to_all | solution.py:69
Sparse Core Ops, SparseCore 0:
  84.4 28.2 all-gather.1
where the time goes:
time: 216 us
  waiting for transfers between devices  80.4 us (37%)
  blocking collectives  80.2 us (37%)
  starting transfers between devices  13.9 us (6%)
  between operations  13.6 us (6%)
  matrix products  11.1 us (5%)
  other arithmetic  9.82 us (5%)
  local copies, waits for them, and re-layouts  7.08 us (3%)
    all_to_all x1, blocking collectives, on_device(): lax.all_to_all(outgoing.reshape(expert_count, capacity, part_width), 'ep'...  72 us
    all_to_all x1, waiting for transfers between devices, on_device(): lax.all_to_all(results, 'ep', split_axis=0, concat_axis=0, tiled=True)  51.9 us
    all_gather x1, waiting for transfers between devices, on_device(): column_piece = lax.all_gather(arrived, 'tp', axis=1, tiled=True)  28.4 us
    all_to_all x1, starting transfers between devices, on_device(): lax.all_to_all(results, 'ep', split_axis=0, concat_axis=0, tiled=True)  13.9 us
    all_to_all x1, blocking collectives, sum_at_owner(): blocks = lax.all_to_all(cut_along(array, dim, size), axis, 0, 0, tiled=True)  8.19 us
    dot_general x1, matrix products, on_device(): jnp.dot(column_piece, up_local, preferred_element_type=jnp.float32)  5.32 us
    reduce_sum x1, other arithmetic, sum_at_owner(): return jnp.sum(blocks.astype(jnp.float32), axis=0)  5.22 us
    gather x1, local copies, waits for them, and re-layouts, on_device(): returned[slot_index].astype(jnp.float32)  4.59 us
  transfers between devices with their start and end apart: 2, of which 2 were waited for; matrix products, arithmetic and copies ran while one was open for 0% of the time, Pallas kernels for 0%

commit v1 on v0

--- a/solution.py
+++ b/solution.py
@@ -6,6 +6,11 @@
 TOP = 8
 EXP_GRP = 8
 EPSILON = 1e-06
+
+
+def skins_answer(chunk, dim_i):
+    z = jnp.concatenate([chunk for _ in range(lax.axis_size("tp"))], dim_i)
+    return lax.all_to_all(z, split_axis=dim_i, axis_name="tp", concat_axis=dim_i, tiled=True)
 
 
 def cut_along(array, dim, size):
@@ -57,7 +62,7 @@
         tiled=True,
     )
     arrived = arrived.reshape(slot_total, part_width)
-    column_piece = lax.all_gather(arrived, "tp", axis=1, tiled=True)
+    column_piece = skins_answer(arrived, 1)
     gate_acts = jnp.dot(column_piece, gate_local, preferred_element_type=jnp.float32)
     up_acts = jnp.dot(column_piece, up_local, preferred_element_type=jnp.float32)
     hidden = (jax.nn.silu(gate_acts) * up_acts).astype(jnp.bfloat16)

time: 216 us -> 187 us (0.87); the launches traced: 216 us -> 183 us
  waiting for transfers between devices: 80.4 us -> 52 us
  between operations: 13.6 us -> 0.18 us
  blocking collectives: 80.2 us -> 88.1 us
  local copies, waits for them, and re-layouts: 7.08 us -> 13.3 us
  starting transfers between devices: 13.9 us -> 8.42 us
    all_gather x1 -> x0, waiting for transfers between devices: 28.4 us -> none  [on_device(): column_piece = lax.all_gather(arrived, 'tp', axis=1, tiled=True)]
    all_to_all x0 -> x1, blocking collectives: none -> 8.19 us  [skins_answer(): lax.all_to_all(z, split_axis=dim_i, axis_name='tp', concat_axis=dim_i, ti...]
    all_to_all x0 -> x1, local copies, waits for them, and re-layouts: none -> 6.21 us  [skins_answer(): lax.all_to_all(z, split_axis=dim_i, axis_name='tp', concat_axis=dim_i, ti...]
    all_to_all x1, starting transfers between devices: 13.9 us -> 8.42 us  [on_device(): lax.all_to_all(results, 'ep', split_axis=0, concat_axis=0, tiled=True)]
  transfers between devices with their start and end apart: 2 -> 1, of which waited for: 2 -> 1; matrix products, arithmetic and copies ran while one was open for 0% -> 0% of each run, Pallas kernels for 0% -> 0%
where the time goes in v1:
time: 187 us; the launch traced here: 183 us
  blocking collectives  88.1 us (47%)
  waiting for transfers between devices  52 us (28%)
  local copies, waits for them, and re-layouts  13.3 us (7%)
  matrix products  11.2 us (6%)
  other arithmetic  10.2 us (5%)
  starting transfers between devices  8.42 us (5%)
    all_to_all x1, blocking collectives, on_device(): lax.all_to_all(outgoing.reshape(expert_count, capacity, part_width), 'ep'...  71.8 us
    all_to_all x1, waiting for transfers between devices, on_device(): lax.all_to_all(results, 'ep', split_axis=0, concat_axis=0, tiled=True)  52 us
    all_to_all x1, starting transfers between devices, on_device(): lax.all_to_all(results, 'ep', split_axis=0, concat_axis=0, tiled=True)  8.42 us
    all_to_all x1, blocking collectives, sum_at_owner(): blocks = lax.all_to_all(cut_along(array, dim, size), axis, 0, 0, tiled=True)  8.19 us
    all_to_all x1, blocking collectives, skins_answer(): lax.all_to_all(z, split_axis=dim_i, axis_name='tp', concat_axis=dim_i, ti...  8.19 us
    all_to_all x1, local copies, waits for them, and re-layouts, skins_answer(): lax.all_to_all(z, split_axis=dim_i, axis_name='tp', concat_axis=dim_i, ti...  6.21 us
    dot_general x1, matrix products, on_device(): jnp.dot(column_piece, up_local, preferred_element_type=jnp.float32)  5.36 us
    reduce_sum x1, other arithmetic, sum_at_owner(): return jnp.sum(blocks.astype(jnp.float32), axis=0)  5.22 us
  transfers between devices with their start and end apart: 1, of which 1 were waited for; matrix products, arithmetic and copies ran while one was open for 0% of the time, Pallas kernels for 0%

profile of v1, /device:TPU:514, one launch (start us, length us, event | category | flops | bytes accessed | tf_op | source)
XLA Modules:
  0.0 183.4 jit_solution(10522812720829425600)
XLA Ops:
  0.0 0.0 copy-start
  0.0 1.1 convert_element_type.40
  1.1 1.1 multiply_reduce_fusion
  2.3 0.8 copy.32
  3.0 0.1 eq.43
  3.1 0.3 convert_reduce_fusion.1
  3.4 0.1 reduce_sum.71
  3.5 0.7 convert_reduce_fusion
  4.2 0.7 dynamic-slice
  4.9 0.8 convolution_convert_fusion.1
  5.6 71.8 %all_to_all.24 = bf16[64,16,1024]{2,1,0:T(8,128)(2,1)S(1)} all-to-all(bf16[64,16,1024]{2,1,0:T(8,128)(2,1)S(1)} %bitcast.36), channel_id=1, replica_groups=mesh['grp'=2,'ep'=64,'tp'=2] {'ep'}, dimensions={0} | all-to-all | bytes 4194304 | tf_op jit(solution)/shard_map/all_to_all | solution.py:57
  77.4 0.4 pad_maximum_fusion
  77.8 8.2 %all_to_all.25 = bf16[1024,2,1024]{2,0,1:T(8,128)(2,1)} all-to-all(bf16[1024,2,1024]{2,0,1:T(8,128)(2,1)S(1)} %pad_maximum_fusion), channel_id=1, replica_groups=mesh['grp'=2,'ep'=64,'tp'=2] {'tp'}, dimensions={1} | all-to-all | bytes 8388608 | tf_op jit(solution)/shard_map/all_to_all | solution.py:13
  86.0 6.2 %copy.34 = bf16[1024,2,1024]{0,2,1:T(8,128)(2,1)} copy(bf16[1024,2,1024]{2,0,1:T(8,128)(2,1)} %all_to_all.25) | data formatting | bytes 8388608 | tf_op jit(solution)/shard_map/all_to_all | solution.py:13
  92.2 5.4 %fusion.2 = f32[1024,512]{1,0:T(8,128)S(1)} fusion(bf16[1024,2048]{0,1:T(8,128)(2,1)} %bitcast.32, bf16[1,2048,512]{2,1,0:T(8,128)(2,1)} %param.11), kind=kOutput, calls=%fused_computation.7 | convolution fusion | flops 2147483648 | bytes 8388608 | tf_op jit(solution)/shard_map/dot_general | solution.py:67
  97.5 0.0 copy-done.1
  97.6 0.0 copy-done.5
  97.6 2.7 %multiply_convert_fusion = bf16[1024,512]{1,0:T(8,128)(2,1)S(1)} fusion(f32[1024,512]{1,0:T(8,128)S(1)} %fusion.2, bf16[1024,2048]{0,1:T(8,128)(2,1)S(1)} %bitcast.33, bf16[1,2048,512]{2,1,0:T(8,128)(2,1)S(1)} %copy-done.5), kind=kOutput, calls=%fused_computation.11 | convolution fusion | flops 2150629376 | bytes 9437184 | tf_op jit(solution)/shard_map/dot_general | solution.py:66
  100.3 0.0 copy-done
  100.3 2.4 %convolution_convert_fusion = bf16[64,16,2048]{2,1,0:T(8,128)(2,1)S(1)} fusion(bf16[64,16,512]{2,1,0:T(8,128)(2,1)S(1)} %bitcast.40, bf16[1,512,2048]{2,1,0:T(8,128)(2,1)S(1)} %copy-done), kind=kOutput, calls=%fused_computation.3 | convolution fusion | flops 2149580800 | bytes 7340032 | tf_op jit(solution)/shard_map/dot_general | solution.py:69
  102.7 0.6 copy.39
  103.3 8.2 %all_to_all.26 = bf16[2,64,16,1024]{3,2,1,0:T(8,128)(2,1)} all-to-all(bf16[2,64,16,1024]{3,2,1,0:T(8,128)(2,1)S(1)} %bitcast.34), channel_id=1, replica_groups=mesh['grp'=2,'ep'=64,'tp'=2] {'tp'}, dimensions={0} | all-to-all | bytes 8388608 | tf_op jit(solution)/shard_map/all_to_all | solution.py:24
  111.5 5.2 %reduce_sum.74 = bf16[64,16,1024]{2,1,0:T(8,128)(2,1)} reduce(bf16[2,64,16,1024]{3,2,1,0:T(8,128)(2,1)} %all_to_all.26, bf16[]{:T(256)} %constant.37.clone.1), dimensions={0}, to_apply=%region_3.4 | reduce | flops 1048576 | bytes 6291458 | tf_op jit(solution)/shard_map/reduce_sum | solution.py:25
  116.7 8.4 %all-to-all-start.3 = ((bf16[64,16,1024]{2,1,0:T(8,128)(2,1)}), bf16[64,16,1024]{2,1,0:T(8,128)(2,1)}, u32[]{:S(2)}, u32[]{:S(2)}) async-start(bf16[64,16,1024]{2,1,0:T(8,128)(2,1)} %reduce_sum.74), calls=%async_computation.3 | async-start | bytes 4194304 | tf_op jit(solution)/shard_map/all_to_all | solution.py:74
  125.2 0.1 mul.78
  125.2 0.0 copy-done.2
  125.3 0.0 copy-done.3
  125.3 0.0 copy-done.4
  125.3 0.1 copy.36
  125.4 52.0 %all-to-all-done.3 = bf16[64,16,1024]{2,1,0:T(8,128)(2,1)} async-done(((bf16[64,16,1024]{2,1,0:T(8,128)(2,1)}), bf16[64,16,1024]{2,1,0:T(8,128)(2,1)}, u32[]{:S(2)}, u32[]{:S(2)}) %all-to-all-start.3) | async-done | bytes 2097184 | tf_op jit(solution)/shard_map/all_to_all | solution.py:74
  177.5 4.6 %gather_fusion = bf16[512,1024]{1,0:T(8,128)(2,1)S(1)} fusion(bf16[1024,1024]{1,0:T(8,128)(2,1)} %bitcast.9, s32[1024]{0:T(1024)S(1)} %pad_clamp_fusion), kind=kCustom, calls=%fused_computation | custom fusion | bytes 2099200 | tf_op jit(solution)/shard_map/gather | solution.py:77
  182.1 1.3 fusion
  (13 shorter events, 0.1 us)
Async XLA Ops:
  0.0 100.3 %copy-start = (bf16[1,512,2048]{2,1,0:T(8,128)(2,1)S(1)}, bf16[1,512,2048]{2,1,0:T(8,128)(2,1)}, u32[]{:S(2)}) copy-start(bf16[1,512,2048]{2,1,0:T(8,128)(2,1)} %param.12) | copy-start | bytes 6291460
  92.2 5.4 %copy-start.1 = (bf16[1024,2,1024]{0,2,1:T(8,128)(2,1)S(1)}, bf16[1024,2,1024]{0,2,1:T(8,128)(2,1)}, u32[]{:S(2)}) copy-start(bf16[1024,2,1024]{0,2,1:T(8,128)(2,1)} %copy.34) | copy-start | bytes 12582916
  92.2 5.4 %copy-start.5 = (bf16[1,2048,512]{2,1,0:T(8,128)(2,1)S(1)}, bf16[1,2048,512]{2,1,0:T(8,128)(2,1)}, u32[]{:S(2)}) copy-start(bf16[1,2048,512]{2,1,0:T(8,128)(2,1)} %param.10) | copy-start | bytes 6291460
  116.7 8.5 %copy-start.2 = (f32[64,8]{0,1:T(8,128)S(1)}, f32[64,8]{0,1:T(8,128)}, u32[]{:S(2)}) copy-start(f32[64,8]{0,1:T(8,128)} %param.15) | copy-start | bytes 6148
  116.7 8.6 %copy-start.3 = (s32[64,8]{0,1:T(8,128)S(1)}, s32[64,8]{0,1:T(8,128)}, u32[]{:S(2)}) copy-start(s32[64,8]{0,1:T(8,128)} %param.13) | copy-start | bytes 6148
  116.7 8.6 %copy-start.4 = (f32[64,8]{0,1:T(8,128)S(1)}, f32[64,8]{0,1:T(8,128)}, u32[]{:S(2)}) copy-start(f32[64,8]{0,1:T(8,128)} %param.14) | copy-start | bytes 6148
  116.7 60.8 %all-to-all-start.3 = ((bf16[64,16,1024]{2,1,0:T(8,128)(2,1)}), bf16[64,16,1024]{2,1,0:T(8,128)(2,1)}, u32[]{:S(2)}, u32[]{:S(2)}) async-start(bf16[64,16,1024]{2,1,0:T(8,128)(2,1)} %reduce_sum.74), calls=%async_computation.3 | async-start | bytes 4194304 | tf_op jit(solution)/shard_map/all_to_all | solution.py:74
